TPU v7x, 32 devices: a whole 2x2x4 slice. The times are simulated.
32 devices in a mesh: fs: 16 (over z, y, x), tp: 2 (over core).
Axes of the slice: x: 2, y: 2, z: 4, core: 2. Of those that a mesh axis runs over, the one named last changes fastest.
Arguments:
- tokens: bfloat16 [6144, 2048], P('fs', 'tp'), may hold values from -24 to 24, as said below
- mixer_gain: float32 [2048], replicated, may hold values from 0.1 to 1.9
- w_content: float32 [2048, 1024], P('fs', 'tp'), may hold values from -0.125 to 0.125
- w_spatial: float32 [2048, 1024], P('fs', 'tp'), may hold values from -0.125 to 0.125
- content_scale: float32 [1024], P('tp'), may hold values from 0.5 to 2
- spatial_scale: float32 [1024], P('tp'), may hold values from 0.2 to 3.5, as said below
- spatial_gain: float32 [1024], P('tp'), may hold values from 0.1 to 1.9
- block_mixing: bfloat16 [8, 128, 128], P('tp'), may hold values from -0.5 to 0.5
- block_bias: float32 [8, 128], P('tp'), may hold values from -6 to 6
- w_project: float32 [1024, 2048], P('tp', 'fs'), may hold values from -0.1875 to 0.1875
- project_scale: float32 [2048], P('fs'), may hold values from 0.5 to 2
- channel_gain: float32 [2048], replicated, may hold values from 0.1 to 1.9
- w_up: float32 [2048, 8192], P('fs', 'tp'), may hold values from -0.125 to 0.125
- up_scale: float32 [8192], P('tp'), may hold values from 0.5 to 2
- w_down: float32 [8192, 2048], P('tp', 'fs'), may hold values from -0.0625 to 0.0625
- down_scale: float32 [2048], P('fs'), may hold values from 0.5 to 2
Outputs:
- layer_out: bfloat16 [6144, 2048], P('fs', 'tp')
Inputs may be any that keep to these rules, and one draw needn't show every extreme that they name: `tokens`: activations whose features and rows have differing scales. `spatial_scale`: positive column scales.
All inputs are finite; a program needn't handle non-finite values.
Results may differ from a plain program's by a relative error of at most 0.019.
Values may be sent and summed in bfloat16 or wider, within the bound.
A program may use at most 128 MiB of HBM per device.

v0:
```python
import functools

import jax
import jax.numpy as jnp
from jax import lax
from jax.experimental import pallas as pl
from jax.experimental.pallas import tpu as pltpu
from jax.sharding import PartitionSpec as P

EPSILON = 1e-06


def normalize_rows(token_rows, gain_vector):
    values = token_rows.astype(jnp.float32)
    scaled = values * lax.rsqrt(jnp.mean(values * values, axis=-1, keepdims=True) + EPSILON)
    return (scaled * gain_vector).astype(jnp.bfloat16)


def shards(
    tokens,
    mixer_gain,
    w_content,
    w_spatial,
    content_scale,
    spatial_scale,
    spatial_gain,
    block_mixing,
    block_bias,
    w_project,
    project_scale,
    channel_gain,
    w_up,
    up_scale,
    w_down,
    down_scale,
):
    content_weight = w_content.astype(jnp.bfloat16)
    spatial_weight = w_spatial.astype(jnp.bfloat16)
    project_weight = w_project.astype(jnp.bfloat16)
    up_weight = w_up.astype(jnp.bfloat16)
    down_weight = w_down.astype(jnp.bfloat16)
    project_full, down_full = (
        lax.all_gather(project_scale, "fs", axis=0, tiled=True),
        lax.all_gather(down_scale, "fs", axis=0, tiled=True),
    )
    gathered_rows = lax.all_gather(tokens, "tp", axis=1, tiled=True)
    normed = normalize_rows(gathered_rows, mixer_gain)
    row_count = gathered_rows.shape[0]
    content_full, spatial_full, project_cols = (
        lax.all_gather(content_weight, "fs", axis=0, tiled=True),
        lax.all_gather(spatial_weight, "fs", axis=0, tiled=True),
        lax.all_gather(project_weight, "fs", axis=1, tiled=True),
    )
    content_linear = jnp.dot(normed, content_full, preferred_element_type=jnp.float32)
    spatial_linear = jnp.dot(normed, spatial_full, preferred_element_type=jnp.float32)
    content = jax.nn.gelu(content_linear * content_scale)
    spatial = jax.nn.gelu(spatial_linear * spatial_scale)
    square_sums = lax.psum(jnp.sum(spatial * spatial, axis=1), "tp")
    total_width = spatial.shape[1] * lax.axis_size("tp")
    spatial_norm = (
        spatial * lax.rsqrt(square_sums / total_width + EPSILON)[:, None] * spatial_gain
    ).astype(jnp.bfloat16)
    groups_here = block_mixing.shape[0]
    block_size = block_mixing.shape[1]
    group_width = spatial_norm.shape[1] // groups_here
    causal_mask = jnp.tril(jnp.ones((block_size, block_size), dtype=bool))
    mixing_weights = jnp.where(causal_mask[None, :, :], block_mixing, jnp.zeros_like(block_mixing))
    grouped = spatial_norm.reshape(row_count // block_size, block_size, groups_here, group_width)
    mixed_block = (
        jnp.einsum("gts,nsgc->ntgc", mixing_weights, grouped, preferred_element_type=jnp.float32)
        + block_bias.T[None, :, :, None]
    )
    gated = (content * mixed_block.reshape(row_count, spatial_norm.shape[1])).astype(jnp.bfloat16)
    mixer_terms = jnp.dot(gated, project_cols, preferred_element_type=jnp.float32) * project_full
    mixer_sum = lax.psum_scatter(
        mixer_terms.astype(jnp.bfloat16), "tp", scatter_dimension=1, tiled=True
    ).astype(jnp.float32)
    middle = (tokens.astype(jnp.float32) + mixer_sum).astype(jnp.bfloat16)
    middle_rows = lax.all_gather(middle, "tp", axis=1, tiled=True)
    channel_normed = normalize_rows(middle_rows, channel_gain)
    up_full, down_cols = (
        lax.all_gather(up_weight, "fs", axis=0, tiled=True),
        lax.all_gather(down_weight, "fs", axis=1, tiled=True),
    )
    up_linear = jnp.dot(channel_normed, up_full, preferred_element_type=jnp.float32)
    hidden = jnp.square(jax.nn.relu(up_linear * up_scale)).astype(jnp.bfloat16)
    channel_terms = jnp.dot(hidden, down_cols, preferred_element_type=jnp.float32) * down_full
    channel_sum = lax.psum_scatter(
        channel_terms.astype(jnp.bfloat16), "tp", scatter_dimension=1, tiled=True
    ).astype(jnp.float32)
    return (middle.astype(jnp.float32) + channel_sum).astype(jnp.bfloat16)


PLANE = 4
MESH = pl.DeviceIdType.MESH


def layer_kernel(
    sizes,
    tokens_ref,
    mixer_gain_ref,
    content_ref,
    spatial_ref,
    content_scale_ref,
    spatial_scale_ref,
    spatial_gain_ref,
    mixing_ref,
    bias_ref,
    project_ref,
    project_scale_ref,
    channel_gain_ref,
    up_hbm,
    up_scale_ref,
    down_hbm,
    down_scale_ref,
    out_ref,
    up_ref,
    down_ref,
    load_sem,
    token_rows,
    normed,
    gate_weights,
    project_full,
    up_own,
    down_own,
    up_full,
    down_full,
    content_buf,
    spatial_buf,
    gated,
    sums,
    sums_in,
    part,
    part_in,
    middle,
    rows_all,
    hidden,
    terms,
    terms_in,
    results_in,
    pair_send,
    pair_recv,
    swap_send,
    swap_recv,
    line_send,
    line_recv,
    gate_line_send,
    gate_line_recv,
    gate_send,
    gate_recv,
    row_send,
    row_recv,
    fwd_send,
    fwd_recv,
    term_send,
    term_recv,
    result_send,
    result_recv,
):
    lines = sizes["lines"]
    rows, half = tokens_ref.shape
    width = token_rows.shape[1]
    depth = content_ref.shape[0]
    channels = content_ref.shape[1]
    units = up_full.shape[1]
    band = PLANE * depth
    chunk = sizes["chunk"]
    me = lax.axis_index("fs")
    core = lax.axis_index("tp")
    z = me // PLANE
    p = me % PLANE
    other = 1 - core
    f32, bf16 = jnp.float32, jnp.bfloat16

    def span(start, size, by=128):
        return pl.ds(pl.multiple_of(start, by), size)

    def peer(k):
        return (p + k) % PLANE

    def on_plane(k):
        return {"fs": z * PLANE + peer(k)}

    pair = {"tp": other}

    def remote(src, dst, send, recv, where):
        return pltpu.make_async_remote_copy(
            src_ref=src, dst_ref=dst, send_sem=send, recv_sem=recv, device_id=where, device_id_type=MESH
        )

    loads = [
        pltpu.make_async_copy(up_hbm, up_ref, load_sem.at[0]),
        pltpu.make_async_copy(down_hbm, down_ref, load_sem.at[1]),
    ]
    for load in loads:
        load.start()
    barrier = pltpu.get_barrier_semaphore()
    for k in range(1, PLANE):
        pl.semaphore_signal(barrier, inc=1, device_id=on_plane(k), device_id_type=MESH)
    pl.semaphore_signal(barrier, inc=1, device_id=pair, device_id_type=MESH)

    @pl.when(z > 0)
    def _():
        pl.semaphore_signal(barrier, inc=1, device_id={"fs": me - PLANE}, device_id_type=MESH)

    @pl.when(z < lines - 1)
    def _():
        pl.semaphore_signal(barrier, inc=1, device_id={"fs": me + PLANE}, device_id_type=MESH)

    gate_weights[span(me * depth, depth), pl.ds(0, channels)] = content_ref[...].astype(bf16)
    gate_weights[span(me * depth, depth), pl.ds(channels, channels)] = spatial_ref[...].astype(bf16)
    project_full[:, span(me * depth, depth)] = (project_ref[...] * project_scale_ref[...]).astype(bf16)

    token_rows[:, span(core * half, half)] = tokens_ref[...]

    along = (z > 0).astype(jnp.int32) + (z < lines - 1).astype(jnp.int32)
    pl.semaphore_wait(barrier, PLANE + along)

    def gate_refs(owner):
        return (
            gate_weights.at[span(owner * depth, depth), :],
            project_full.at[:, span(owner * depth, depth)],
        )

    def gate_line(block, side, step):
        refs = gate_refs(block * PLANE + p)
        return [
            remote(
                refs[a], refs[a], gate_line_send.at[a, side, block], gate_line_recv.at[a, block],
                {"fs": me + step * PLANE},
            )
            for a in range(2)
        ]

    def gate_plane(block, k):
        refs = gate_refs(block * PLANE + p)
        return [
            remote(refs[a], refs[a], gate_send.at[a, block, k], gate_recv.at[a, block, k], on_plane(k))
            for a in range(2)
        ]

    def ff_line(a, block, side, step):
        ref = up_full.at[span(block * band, band), :] if a == 0 else down_full.at[:, span(block * band, band)]
        return remote(
            ref, ref, line_send.at[a, side, block], line_recv.at[a, block], {"fs": me + step * PLANE}
        )

    def swap(a, k):
        if a == 0:
            src = up_own.at[:, span(peer(k) * units, units)]
            dst = up_full.at[span(me * depth, depth), :]
        else:
            src = down_own.at[span(peer(k) * units, units), :]
            dst = down_full.at[:, span(me * depth, depth)]
        return remote(src, dst, swap_send.at[a, k], swap_recv.at[a, k], on_plane(k))

    def swap_arrival(a, k):
        owner = z * PLANE + (p + PLANE - k) % PLANE
        dst = up_full.at[span(owner * depth, depth), :] if a == 0 else down_full.at[:, span(owner * depth, depth)]
        return remote(dst, dst, swap_send.at[a, k], swap_recv.at[a, k], on_plane(k))

    def both_sides(block, make):
        @pl.when(z < lines - 1)
        def _():
            make(block, 0, 1)

        @pl.when(z > 0)
        def _():
            make(block, 1, -1)

    def start_gate(block, side, step):
        for copy in gate_line(block, side, step):
            copy.start()

    token_copy = remote(
        tokens_ref, token_rows.at[:, span(core * half, half)], pair_send.at[0], pair_recv.at[0], pair
    )
    token_copy.start()
    both_sides(z, start_gate)
    for load in loads:
        load.wait()

    @pl.loop(0, up_own.shape[1] // units)
    def _(j):
        up_own[:, span(j * units, units)] = up_ref[:, span(j * units, units)].astype(bf16)
        down_own[span(j * units, units), :] = (
            down_ref[span(j * units, units), :] * down_scale_ref[...]
        ).astype(bf16)

    up_full[span(me * depth, depth), :] = up_ref[:, span(p * units, units)].astype(bf16)
    down_full[:, span(me * depth, depth)] = (
        down_ref[span(p * units, units), :] * down_scale_ref[...]
    ).astype(bf16)
    for a in range(2):
        for k in range(1, PLANE):
            swap(a, k).start()
    for k in range(1, PLANE):
        for copy in gate_plane(z, k):
            copy.start()

    token_copy.wait()

    def normalize(source, gain_ref, target, first):
        @pl.loop(0, rows // chunk)
        def _(i):
            values = source[span(i * chunk, chunk, chunk), :].astype(f32)
            scaled = values * lax.rsqrt(jnp.mean(values * values, axis=-1, keepdims=True) + EPSILON)
            target[span(first + i * chunk, chunk, chunk), :] = (scaled * gain_ref[...]).astype(bf16)

    normalize(token_rows, mixer_gain_ref, normed, 0)

    for d in range(1, lines):
        for side, step in ((0, 1), (1, -1)):
            block = z - step * d

            @pl.when((block >= 0) & (block < lines))
            def _(block=block, side=side, step=step):
                for copy in gate_line(block, side, step):
                    copy.wait_recv()

                @pl.when((z + step >= 0) & (z + step < lines))
                def _():
                    start_gate(block, side, step)

                for k in range(1, PLANE):
                    for copy in gate_plane(block, k):
                        copy.start()

    for a in range(2):
        for k in range(1, PLANE):
            swap_arrival(a, k).wait_recv()
        both_sides(z, lambda block, side, step, a=a: ff_line(a, block, side, step).start())

    def relay(d, parts, forward):
        for a in parts:
            for side, step in ((0, 1), (1, -1)):
                block = z - step * d

                @pl.when((block >= 0) & (block < lines))
                def _(a=a, block=block, side=side, step=step):
                    ff_line(a, block, side, step).wait_recv()
                    if forward:

                        @pl.when((z + step >= 0) & (z + step < lines))
                        def _():
                            ff_line(a, block, side, step).start()

    if lines > 2:
        relay(1, (0, 1), True)

    def gate_arrival(block, k):
        refs = gate_refs(block * PLANE + (p + PLANE - k) % PLANE)
        return [
            remote(refs[a], refs[a], gate_send.at[a, block, k], gate_recv.at[a, block, k], on_plane(k))
            for a in range(2)
        ]

    for block in range(lines):
        for k in range(1, PLANE):
            for copy in gate_arrival(block, k):
                copy.wait_recv()

    tile = sizes["tile"]

    @pl.loop(0, channels // tile)
    def _(j):
        at = span(j * tile, tile)
        linear = jnp.dot(normed[...], gate_weights[:, at], preferred_element_type=f32)
        content_buf[:, at] = jax.nn.gelu(linear * content_scale_ref[:, at])
        linear = jnp.dot(
            normed[...], gate_weights[:, span(channels + j * tile, tile)], preferred_element_type=f32
        )
        spatial_buf[:, at] = jax.nn.gelu(linear * spatial_scale_ref[:, at])

    spatial = spatial_buf[...]
    sums[...] = jnp.broadcast_to(jnp.sum(spatial * spatial, axis=1, keepdims=True), sums.shape)
    sum_copy = remote(sums, sums_in, pair_send.at[1], pair_recv.at[1], pair)
    sum_copy.start()
    sum_copy.wait()
    groups, block_size = mixing_ref.shape[0], mixing_ref.shape[1]
    group_width = channels // groups
    causal = lax.broadcasted_iota(jnp.int32, (block_size, block_size), 0) >= lax.broadcasted_iota(
        jnp.int32, (block_size, block_size), 1
    )
    for g in range(groups):
        weights = jnp.where(causal, mixing_ref[g].astype(f32), 0.0).astype(bf16)
        bias = jnp.broadcast_to(bias_ref[pl.ds(g, 1), :], (block_size, block_size)).T[:, :1]
        at = pl.ds(g * group_width, group_width)
        for n in range(rows // block_size):
            these = pl.ds(n * block_size, block_size)
            total = (sums[these, :1] + sums_in[these, :1]) / (2 * channels)
            spatial_norm = (
                spatial_buf[these, at] * lax.rsqrt(total + EPSILON) * spatial_gain_ref[:, at]
            ).astype(bf16)
            mixed = jnp.dot(weights, spatial_norm, preferred_element_type=f32) + bias
            gated[these, at] = (content_buf[these, at] * mixed).astype(bf16)

    @pl.loop(0, width // (2 * tile))
    def _(j):
        at = span(j * 2 * tile, 2 * tile)
        part[:, at] = jnp.dot(gated[...], project_full[:, at], preferred_element_type=f32).astype(bf16)

    part_copy = remote(part.at[:, span(other * half, half)], part_in, pair_send.at[2], pair_recv.at[2], pair)
    part_copy.start()
    part_copy.wait()
    mine = span(core * half, half)

    @pl.loop(0, rows // chunk)
    def _(i):
        these = span(i * chunk, chunk, chunk)
        total = part[these, mine].astype(f32) + part_in[these, :].astype(f32)
        middle[these, mine] = (tokens_ref[these, :].astype(f32) + total).astype(bf16)

    middle_copy = remote(middle.at[:, mine], middle.at[:, mine], pair_send.at[3], pair_recv.at[3], pair)
    middle_copy.start()
    middle_copy.wait()
    normalize(middle, channel_gain_ref, rows_all, p * rows)

    own_rows = rows_all.at[span(p * rows, rows), mine]
    row_copies = [remote(own_rows, own_rows, row_send.at[k], row_recv.at[k], on_plane(k)) for k in range(1, PLANE)]
    for copy in row_copies:
        copy.start()

    for d in range(2, lines - 1):
        relay(d, (0, 1), True)

    forwards = []
    for k in range(1, PLANE):
        theirs = rows_all.at[span((p + PLANE - k) % PLANE * rows, rows), mine]
        remote(theirs, theirs, row_send.at[k], row_recv.at[k], on_plane(k)).wait_recv()
        forwards.append(remote(theirs, theirs, fwd_send.at[k], fwd_recv.at[k], pair))
        forwards[-1].start()
    for copy in forwards:
        copy.wait_recv()

    relay(lines - 1, (0,), False)

    up_tile = sizes["up_tile"]

    @pl.loop(0, PLANE)
    def _(r):
        these = span(r * rows, rows)

        @pl.loop(0, units // up_tile)
        def _(j):
            at = span(j * up_tile, up_tile)
            linear = jnp.dot(rows_all[these, :], up_full[:, at], preferred_element_type=f32)
            linear = linear * up_scale_ref[:, span(p * units + j * up_tile, up_tile)]
            hidden[these, at] = jnp.square(jnp.maximum(linear, 0.0)).astype(bf16)

    per_core = lines // 2

    def result_copy(block, k):
        local = block % per_core
        return remote(
            terms.at[block, span(peer(k) * rows, rows), :],
            results_in.at[k, local],
            result_send.at[local, k],
            result_recv.at[local, k],
            on_plane(k),
        )

    def term_copy(block):
        local = block % per_core
        return remote(terms.at[block], terms_in.at[local], term_send.at[local], term_recv.at[local], pair)

    for i in range(lines):
        block = sizes["order"][0][i]
        for row in range(1, lines):
            block = jnp.where(z == row, sizes["order"][row][i], block)
        if i == lines - 1:
            relay(lines - 1, (1,), False)

        @pl.loop(0, PLANE)
        def _(r, block=block):
            these = span(r * rows, rows)
            terms[block, these, :] = jnp.dot(
                hidden[these, :], down_full[:, span(block * band, band)], preferred_element_type=f32
            ).astype(bf16)

        @pl.when(block // per_core != core)
        def _(block=block):
            term_copy(block).start()

        @pl.when(block // per_core == core)
        def _(block=block):
            term_copy(block).wait_recv()
            local = block % per_core

            @pl.loop(0, PLANE * rows // chunk)
            def _(i):
                these = span(i * chunk, chunk, chunk)
                terms[block, these, :] = (
                    terms[block, these, :].astype(f32) + terms_in[local, these, :].astype(f32)
                ).astype(bf16)

            for k in range(1, PLANE):
                result_copy(block, k).start()

    for i in range(per_core):
        block = core * per_core + i
        for k in range(1, PLANE):
            result_copy(block, k).wait_recv()
        at = pl.ds(i * band, band)

        @pl.loop(0, rows // chunk)
        def _(c, block=block, at=at, i=i):
            these = span(c * chunk, chunk, chunk)
            total = terms[block, span(p * rows + c * chunk, chunk, chunk), :].astype(f32)
            for k in range(1, PLANE):
                total = total + results_in[k, i, these, :].astype(f32)
            out_ref[these, at] = (
                middle[these, span(core * half + i * band, band)].astype(f32) + total
            ).astype(bf16)

    for k in range(1, PLANE):
        for a in range(2):
            swap(a, k).wait_send()
        for block in range(lines):
            for copy in gate_plane(block, k):
                copy.wait_send()
        row_copies[k - 1].wait_send()
        forwards[k - 1].wait_send()
        for i in range(per_core):
            result_copy(core * per_core + i, k).wait_send()
    for i in range(per_core):
        term_copy(other * per_core + i).wait_send()
    for side, step in ((0, 1), (1, -1)):
        for d in range(lines):
            block = z - step * d

            @pl.when((block >= 0) & (block < lines) & (z + step >= 0) & (z + step < lines))
            def _(block=block, side=side, step=step):
                for copy in gate_line(block, side, step):
                    copy.wait_send()
                for a in range(2):
                    ff_line(a, block, side, step).wait_send()


def fused_shards(fs, tokens, mixer_gain, w_content, w_spatial, content_scale, spatial_scale, spatial_gain,
                 block_mixing, block_bias, w_project, project_scale, channel_gain, w_up, up_scale, w_down, down_scale):
    lines = fs // PLANE
    rows, half = tokens.shape
    width = 2 * half
    channels = w_content.shape[1]
    hidden_units = w_up.shape[1]
    units = hidden_units // PLANE
    depth = w_up.shape[0]
    band = PLANE * depth
    per_core = lines // 2
    bf16, f32 = jnp.bfloat16, jnp.float32
    order = [sorted(range(lines), key=lambda b, z=z: (abs(b - z), b)) for z in range(lines)]
    sizes = dict(lines=lines, order=order, chunk=64, tile=256, up_tile=256)
    vmem = pltpu.VMEM
    dma = pltpu.SemaphoreType.DMA
    row = lambda a: a.reshape(1, -1)
    return pl.pallas_call(
        functools.partial(layer_kernel, sizes),
        out_shape=jax.ShapeDtypeStruct((rows, half), bf16),
        in_specs=[
            pl.BlockSpec(memory_space=pl.ANY if i in (12, 14) else vmem) for i in range(16)
        ],
        out_specs=pl.BlockSpec(memory_space=vmem),
        scratch_shapes=[
            vmem((depth, hidden_units), f32),
            vmem((hidden_units, depth), f32),
            dma((2,)),
            vmem((rows, width), bf16),
            vmem((rows, width), bf16),
            vmem((width, 2 * channels), bf16),
            vmem((channels, width), bf16),
            vmem((depth, hidden_units), bf16),
            vmem((hidden_units, depth), bf16),
            vmem((width, units), bf16),
            vmem((units, width), bf16),
            vmem((rows, channels), f32),
            vmem((rows, channels), f32),
            vmem((rows, channels), bf16),
            vmem((rows, 128), f32),
            vmem((rows, 128), f32),
            vmem((rows, width), bf16),
            vmem((rows, half), bf16),
            vmem((rows, width), bf16),
            vmem((PLANE * rows, width), bf16),
            vmem((PLANE * rows, units), bf16),
            vmem((lines, PLANE * rows, band), bf16),
            vmem((per_core, PLANE * rows, band), bf16),
            vmem((PLANE, per_core, rows, band), bf16),
            dma((4,)),
            dma((4,)),
            dma((2, PLANE)),
            dma((2, PLANE)),
            dma((2, 2, lines)),
            dma((2, lines)),
            dma((2, 2, lines)),
            dma((2, lines)),
            dma((2, lines, PLANE)),
            dma((2, lines, PLANE)),
            dma((PLANE,)),
            dma((PLANE,)),
            dma((PLANE,)),
            dma((PLANE,)),
            dma((per_core,)),
            dma((per_core,)),
            dma((per_core, PLANE)),
            dma((per_core, PLANE)),
        ],
        compiler_params=pltpu.CompilerParams(
            collective_id=0, has_side_effects=True, vmem_limit_bytes=VMEM_LIMIT
        ),
    )(tokens, row(mixer_gain), w_content, w_spatial, row(content_scale), row(spatial_scale), row(spatial_gain),
      block_mixing, block_bias, w_project, row(project_scale), row(channel_gain), w_up, row(up_scale), w_down,
      row(down_scale))


VMEM_LIMIT = 67043328


def solution(mesh):
    fs, tp = mesh.shape["fs"], mesh.shape["tp"]
    if tp == 2 and fs % (2 * PLANE) == 0 and fs <= 16:
        body = functools.partial(fused_shards, fs)
    else:
        body = shards
    return jax.shard_map(
        body,
        mesh=mesh,
        in_specs=(
            P("fs", "tp"),
            P(),
            P("fs", "tp"),
            P("fs", "tp"),
            P("tp"),
            P("tp"),
            P("tp"),
            P("tp", None, None),
            P("tp", None),
            P("tp", "fs"),
            P("fs"),
            P(),
            P("fs", "tp"),
            P("tp"),
            P("tp", "fs"),
            P("fs"),
        ),
        out_specs=P("fs", "tp"),
        check_vma=False,
    )
```

profile of v0, /device:TPU:1, one launch (start us, length us, event | category | flops | bytes accessed | tf_op | source)
XLA Modules:
  0.0 204.1 jit_solution(3821672602934845529)
XLA Ops:
  0.0 202.0 %shard_map.154 = bf16[384,1024]{1,0:T(8,128)(2,1)} custom-call(bf16[384,1024]{1,0:T(8,128)(2,1)} %tokens_ref.1, f32[1,2048]{1,0:T(1,128)} %bitcast.9, f32[128,512]{1,0:T(8,128)} %content_ref.1, f32[128,512]{1,0:T(8,128)} %spatial_ref.1, f32[1,512]{1,0:T(1,128)} %bitcast.11, f32[1,512]{1,0:T(1,128)} %bitcast.12, f32[1,512]{1,0:T(1,128)} %bitcast.13, ...), custom_call_target="tpu_custom_call" | custom-call | tf_op jit(solution)/shard_map/pallas_call | solution.py:557
  202.0 2.1 %copy.18 = bf16[384,1024]{1,0:T(8,128)(2,1)} copy(bf16[384,1024]{1,0:T(8,128)(2,1)} %shard_map.154) | data formatting | bytes 1572864
where the time goes:
time: 204 us
  Pallas kernels  202 us (99%)
  local copies, waits for them, and re-layouts  2.06 us (1%)
    pallas_call x1, Pallas kernels, fused_shards(): pl.pallas_call(functools.partial(layer_kernel, sizes), out_shape=jax.Shap...  202 us

commit v1 on v0

v1 whole, which is shorter than its diff:
```python
import functools

import jax
import jax.numpy as jnp
from jax import lax
from jax.experimental import pallas as pl
from jax.experimental.pallas import tpu as pltpu
from jax.sharding import PartitionSpec as P

EPSILON = 1e-06


def normalize_rows(token_rows, gain_vector):
    values = token_rows.astype(jnp.float32)
    scaled = values * lax.rsqrt(jnp.mean(values * values, axis=-1, keepdims=True) + EPSILON)
    return (scaled * gain_vector).astype(jnp.bfloat16)


def shards(
    tokens,
    mixer_gain,
    w_content,
    w_spatial,
    content_scale,
    spatial_scale,
    spatial_gain,
    block_mixing,
    block_bias,
    w_project,
    project_scale,
    channel_gain,
    w_up,
    up_scale,
    w_down,
    down_scale,
):
    content_weight = w_content.astype(jnp.bfloat16)
    spatial_weight = w_spatial.astype(jnp.bfloat16)
    project_weight = w_project.astype(jnp.bfloat16)
    up_weight = w_up.astype(jnp.bfloat16)
    down_weight = w_down.astype(jnp.bfloat16)
    project_full, down_full = (
        lax.all_gather(project_scale, "fs", axis=0, tiled=True),
        lax.all_gather(down_scale, "fs", axis=0, tiled=True),
    )
    gathered_rows = lax.all_gather(tokens, "tp", axis=1, tiled=True)
    normed = normalize_rows(gathered_rows, mixer_gain)
    row_count = gathered_rows.shape[0]
    content_full, spatial_full, project_cols = (
        lax.all_gather(content_weight, "fs", axis=0, tiled=True),
        lax.all_gather(spatial_weight, "fs", axis=0, tiled=True),
        lax.all_gather(project_weight, "fs", axis=1, tiled=True),
    )
    content_linear = jnp.dot(normed, content_full, preferred_element_type=jnp.float32)
    spatial_linear = jnp.dot(normed, spatial_full, preferred_element_type=jnp.float32)
    content = jax.nn.gelu(content_linear * content_scale)
    spatial = jax.nn.gelu(spatial_linear * spatial_scale)
    square_sums = lax.psum(jnp.sum(spatial * spatial, axis=1), "tp")
    total_width = spatial.shape[1] * lax.axis_size("tp")
    spatial_norm = (
        spatial * lax.rsqrt(square_sums / total_width + EPSILON)[:, None] * spatial_gain
    ).astype(jnp.bfloat16)
    groups_here = block_mixing.shape[0]
    block_size = block_mixing.shape[1]
    group_width = spatial_norm.shape[1] // groups_here
    causal_mask = jnp.tril(jnp.ones((block_size, block_size), dtype=bool))
    mixing_weights = jnp.where(causal_mask[None, :, :], block_mixing, jnp.zeros_like(block_mixing))
    grouped = spatial_norm.reshape(row_count // block_size, block_size, groups_here, group_width)
    mixed_block = (
        jnp.einsum("gts,nsgc->ntgc", mixing_weights, grouped, preferred_element_type=jnp.float32)
        + block_bias.T[None, :, :, None]
    )
    gated = (content * mixed_block.reshape(row_count, spatial_norm.shape[1])).astype(jnp.bfloat16)
    mixer_terms = jnp.dot(gated, project_cols, preferred_element_type=jnp.float32) * project_full
    mixer_sum = lax.psum_scatter(
        mixer_terms.astype(jnp.bfloat16), "tp", scatter_dimension=1, tiled=True
    ).astype(jnp.float32)
    middle = (tokens.astype(jnp.float32) + mixer_sum).astype(jnp.bfloat16)
    middle_rows = lax.all_gather(middle, "tp", axis=1, tiled=True)
    channel_normed = normalize_rows(middle_rows, channel_gain)
    up_full, down_cols = (
        lax.all_gather(up_weight, "fs", axis=0, tiled=True),
        lax.all_gather(down_weight, "fs", axis=1, tiled=True),
    )
    up_linear = jnp.dot(channel_normed, up_full, preferred_element_type=jnp.float32)
    hidden = jnp.square(jax.nn.relu(up_linear * up_scale)).astype(jnp.bfloat16)
    channel_terms = jnp.dot(hidden, down_cols, preferred_element_type=jnp.float32) * down_full
    channel_sum = lax.psum_scatter(
        channel_terms.astype(jnp.bfloat16), "tp", scatter_dimension=1, tiled=True
    ).astype(jnp.float32)
    return (middle.astype(jnp.float32) + channel_sum).astype(jnp.bfloat16)


LINES = 4
PLANE = 4
MESH = pl.DeviceIdType.MESH


def layer_kernel(
    sizes,
    tokens_ref,
    mixer_gain_ref,
    content_ref,
    spatial_ref,
    content_scale_ref,
    spatial_scale_ref,
    spatial_gain_ref,
    mixing_ref,
    bias_ref,
    project_ref,
    project_scale_ref,
    channel_gain_ref,
    up_hbm,
    up_scale_ref,
    down_hbm,
    down_scale_ref,
    out_ref,
    up_ref,
    down_ref,
    load_sem,
    token_rows,
    normed,
    gate_weights,
    project_full,
    gate_other,
    project_other,
    up_own,
    down_own,
    up_full,
    down_full,
    content_buf,
    spatial_buf,
    gated,
    sums,
    sums_in,
    part,
    part_in,
    share,
    share_in,
    middle,
    rows_all,
    hidden,
    terms,
    terms_in,
    cross_in,
    line_in,
    token_send,
    token_recv,
    half_send,
    half_recv,
    gate_line_send,
    gate_line_recv,
    gate_send,
    gate_recv,
    swap_send,
    swap_recv,
    across_send,
    across_recv,
    beside_send,
    beside_recv,
    sum_send,
    sum_recv,
    part_send,
    part_recv,
    share_send,
    share_recv,
    middle_send,
    middle_recv,
    row_send,
    row_recv,
    fwd_send,
    fwd_recv,
    term_send,
    term_recv,
    cross_send,
    cross_recv,
    line_send,
    line_recv,
):
    rows, half = tokens_ref.shape
    width = 2 * half
    depth = content_ref.shape[0]
    channels = content_ref.shape[1]
    share_width = channels // 2
    units = up_full.shape[1]
    slab = 2 * depth
    fine = sizes["fine"]
    tile = sizes["tile"]
    groups, block_size = mixing_ref.shape[0], mixing_ref.shape[1]
    blocks = rows // block_size
    steps = rows // block_size
    me = lax.axis_index("fs")
    core = lax.axis_index("tp")
    z = me // PLANE
    p = me % PLANE
    y = p // 2
    x = p % 2
    zh = z // 2
    zl = z % 2
    other = 1 - core
    f32, bf16 = jnp.float32, jnp.bfloat16

    def span(start, size, by=128):
        return pl.ds(pl.multiple_of(start, by), size)

    beside_x = me + 1 - 2 * x
    beside_y = me + 2 - 4 * y
    beside_z = me + PLANE * (1 - 2 * zl)
    corner = beside_z + 1 - 2 * x
    far_z = me + 2 * PLANE * (1 - 2 * zh)
    inner = (z > 0) & (z < LINES - 1)
    pair = {"tp": other}
    mine = span(core * half, half)

    def remote(src, dst, send, recv, where):
        return pltpu.make_async_remote_copy(
            src_ref=src, dst_ref=dst, send_sem=send, recv_sem=recv, device_id=where, device_id_type=MESH
        )

    loads = [
        pltpu.make_async_copy(up_hbm, up_ref, load_sem.at[0]),
        pltpu.make_async_copy(down_hbm, down_ref, load_sem.at[1]),
    ]
    for load in loads:
        load.start()
    barrier = pltpu.get_barrier_semaphore()
    friends = [{"fs": i} for i in (beside_x, beside_y, beside_z, corner, far_z)]
    friends += [pair, {"fs": beside_x, "tp": other}]
    for friend in friends:
        pl.semaphore_signal(barrier, inc=1, device_id=friend, device_id_type=MESH)

    @pl.when(inner)
    def _():
        pl.semaphore_signal(
            barrier, inc=1, device_id={"fs": me + PLANE * (2 * zl - 1)}, device_id_type=MESH
        )

    own_channels = span(x * share_width, share_width)
    own_depth = span(me * depth, depth)

    def halves(channel_half, weights, project):
        at = span(channel_half * share_width, share_width)
        weights[:, pl.ds(0, share_width)] = content_ref[:, at].astype(bf16)
        weights[:, pl.ds(share_width, share_width)] = spatial_ref[:, at].astype(bf16)
        project[...] = (project_ref[at, :] * project_scale_ref[...]).astype(bf16)

    halves(1 - x, gate_other, project_other)
    halves(x, gate_weights.at[own_depth, :], project_full.at[:, own_depth])
    token_rows[0, :, mine] = tokens_ref[...]
    pl.semaphore_wait(barrier, len(friends) + inner.astype(jnp.int32))

    def slab_at(q, yy):
        return span((q * PLANE + yy * 2) * depth, slab)

    def gate_refs(q, yy):
        at = slab_at(q, yy)
        return gate_weights.at[at, :], project_full.at[:, at]

    def gate_line(q, side, step):
        refs = gate_refs(q, y)
        return [
            remote(
                refs[a], refs[a], gate_line_send.at[a, side, q], gate_line_recv.at[a, q],
                {"fs": me + step * PLANE},
            )
            for a in range(2)
        ]

    def gate_cross(q, yy):
        refs = gate_refs(q, yy)
        return [
            remote(refs[a], refs[a], gate_send.at[a, q], gate_recv.at[a, q], {"fs": beside_y}) for a in range(2)
        ]

    half_copies = [
        remote(gate_other, gate_weights.at[own_depth, :], half_send.at[0], half_recv.at[0], {"fs": beside_x}),
        remote(project_other, project_full.at[:, own_depth], half_send.at[1], half_recv.at[1], {"fs": beside_x}),
    ]

    swap_to = (beside_x, beside_z, corner)
    swap_part = (2 * zl + 1 - x, 2 * (1 - zl) + x, 2 * (1 - zl) + 1 - x)

    def swap(a, k):
        theirs = span(swap_part[k] * units, units)
        src = up_own.at[:, theirs] if a == 0 else down_own.at[theirs, :]
        dst = up_full.at[own_depth, :] if a == 0 else down_full.at[:, own_depth]
        return remote(src, dst, swap_send.at[a, k], swap_recv.at[a, k], {"fs": swap_to[k]})

    def ff_ref(a, q, yy):
        return up_full.at[slab_at(q, yy), :] if a == 0 else down_full.at[:, slab_at(q, yy)]

    def line_of(g, b):
        return 2 * (zh if g == 0 else 1 - zh) + b

    def across(a, b):
        ref = ff_ref(a, line_of(0, b), y)
        return remote(ref, ref, across_send.at[a, b], across_recv.at[a, b], {"fs": far_z})

    def beside(a, g, b):
        ref = ff_ref(a, line_of(g, b), y)
        return remote(ref, ref, beside_send.at[a, g, b], beside_recv.at[a, g, b], {"fs": beside_y})

    def relay_gate(d):
        for side, step in ((0, 1), (1, -1)):
            q = z - step * d

            @pl.when((q >= 0) & (q < LINES))
            def _(q=q, side=side, step=step):
                for copy in gate_line(q, side, step):
                    copy.wait_recv()

                @pl.when((z + step >= 0) & (z + step < LINES))
                def _():
                    for copy in gate_line(q, side, step):
                        copy.start()

                for copy in gate_cross(q, y):
                    copy.start()

    for copy in half_copies:
        copy.start()
    token_pair = remote(tokens_ref, token_rows.at[0, :, mine], token_send.at[0], token_recv.at[0], pair)
    token_pair.start()
    for load in loads:
        load.wait()

    @pl.loop(0, up_own.shape[1] // units)
    def _(j):
        up_own[:, span(j * units, units)] = up_ref[:, span(j * units, units)].astype(bf16)

    quarter = span((2 * zl + x) * units, units)
    swap(0, 0).start()
    token_cross = remote(
        tokens_ref, token_rows.at[1, :, mine], token_send.at[1], token_recv.at[1], {"fs": beside_x}
    )
    token_cross.start()
    up_full[own_depth, :] = up_ref[:, quarter].astype(bf16)

    @pl.loop(0, up_own.shape[1] // units)
    def _(j):
        down_own[span(j * units, units), :] = (
            down_ref[span(j * units, units), :] * down_scale_ref[...]
        ).astype(bf16)

    down_full[:, own_depth] = (down_ref[quarter, :] * down_scale_ref[...]).astype(bf16)

    for copy in half_copies:
        copy.wait_recv()
    for side, step in ((0, 1), (1, -1)):

        @pl.when((z + step >= 0) & (z + step < LINES))
        def _(side=side, step=step):
            for copy in gate_line(z, side, step):
                copy.start()

    for copy in gate_cross(z, y):
        copy.start()
    swap(0, 1).start()
    swap(0, 2).start()

    def normalize(source, gain_ref, target, first, count):
        @pl.loop(0, count // fine)
        def _(i):
            these = span(first + i * fine, fine, fine)
            values = source[these, :].astype(f32)
            scaled = values * lax.rsqrt(jnp.mean(values * values, axis=-1, keepdims=True) + EPSILON)
            target[these, :] = (scaled * gain_ref[...]).astype(bf16)

    token_pair.wait()
    normalize(token_rows.at[0], mixer_gain_ref, normed.at[0], 0, rows)
    relay_gate(1)
    relay_gate(2)
    for k in range(3):
        swap(1, k).start()
    for k in range(3):
        swap(0, k).wait_recv()
    for b in range(2):
        across(0, b).start()
    relay_gate(3)
    for b in range(2):
        beside(0, 0, b).start()

    token_cross.wait()
    token_forward = remote(
        token_rows.at[1, :, mine], token_rows.at[1, :, mine], token_send.at[2], token_recv.at[2], pair
    )
    token_forward.start()
    token_forward.wait()
    normalize(token_rows.at[1], mixer_gain_ref, normed.at[1], 0, rows)

    for q in range(LINES):
        for copy in gate_cross(q, 1 - y):
            copy.wait_recv()

    @pl.loop(0, 2)
    def _(s):
        linear = jnp.dot(normed[s], gate_weights[:, pl.ds(share_width, share_width)], preferred_element_type=f32)
        spatial_buf[s] = jax.nn.gelu(linear * spatial_scale_ref[:, own_channels])

    sums[...] = jnp.zeros_like(sums)
    for s in range(2):
        for n in range(blocks):
            values = spatial_buf[s, pl.ds(n * block_size, block_size), :]
            total = jnp.sum(values * values, axis=1, keepdims=True)
            sums[pl.ds(s * blocks + n, 1), :] = jnp.broadcast_to(total, (block_size, block_size)).T[:1, :]
    sum_to = (pair, {"fs": beside_x}, {"fs": beside_x, "tp": other})
    sum_copies = [remote(sums, sums_in.at[k], sum_send.at[k], sum_recv.at[k], sum_to[k]) for k in range(3)]
    for copy in sum_copies:
        copy.start()

    @pl.loop(0, 2)
    def _(s):
        linear = jnp.dot(normed[s], gate_weights[:, pl.ds(0, share_width)], preferred_element_type=f32)
        content_buf[s] = jax.nn.gelu(linear * content_scale_ref[:, own_channels])

    for copy in sum_copies:
        copy.wait_recv()

    causal = lax.broadcasted_iota(jnp.int32, (block_size, block_size), 0) >= lax.broadcasted_iota(
        jnp.int32, (block_size, block_size), 1
    )
    own_groups = groups // 2
    group_width = channels // groups
    part_copies = [
        remote(
            part.at[s, :, span(other * half, half)], part_in.at[s], part_send.at[s], part_recv.at[s], pair
        )
        for s in range(2)
    ]
    for s in (1, 0):
        for n in range(blocks):
            these = pl.ds(n * block_size, block_size)
            here, there = pl.ds(s * blocks + n, 1), pl.ds((1 - s) * blocks + n, 1)
            total = (sums[here, :] + sums_in[0, here, :]) + (sums_in[1, there, :] + sums_in[2, there, :])
            scale = lax.rsqrt(total / (2 * channels) + EPSILON)
            scale = jnp.broadcast_to(scale, (block_size, block_size)).T[:, :1]
            for g in range(own_groups):
                group = x * own_groups + g
                weights = jnp.where(causal, mixing_ref[group].astype(f32), 0.0).astype(bf16)
                bias = jnp.broadcast_to(bias_ref[pl.ds(group, 1), :], (block_size, block_size)).T[:, :1]
                at = pl.ds(g * group_width, group_width)
                gain = spatial_gain_ref[:, span(group * group_width, group_width)]
                spatial_norm = (spatial_buf[s, these, at] * scale * gain).astype(bf16)
                mixed = jnp.dot(weights, spatial_norm, preferred_element_type=f32) + bias
                gated[s, these, at] = (content_buf[s, these, at] * mixed).astype(bf16)

        @pl.loop(0, width // (2 * tile))
        def _(j, s=s):
            at = span(j * 2 * tile, 2 * tile)
            part[s, :, at] = jnp.dot(gated[s], project_full[:, at], preferred_element_type=f32).astype(bf16)

        part_copies[s].start()

    def step_rows(i):
        return pl.ds(i * block_size, block_size)

    share_copies = [
        remote(
            share.at[step_rows(i), :], share_in.at[step_rows(i), :], share_send.at[i], share_recv.at[i],
            {"fs": beside_x},
        )
        for i in range(steps)
    ]
    part_copies[1].wait_recv()
    for i in range(steps):
        these = step_rows(i)
        share[these, :] = (part[1, these, mine].astype(f32) + part_in[1, these, :].astype(f32)).astype(bf16)
        share_copies[i].start()
    part_copies[0].wait_recv()

    for k in range(3):
        swap(1, k).wait_recv()
    for b in range(2):
        across(1, b).start()
    across(0, 0).wait_recv()
    beside(0, 1, 0).start()
    beside(1, 0, 0).start()

    middle_copies = [
        remote(
            middle.at[step_rows(i), mine], middle.at[step_rows(i), mine], middle_send.at[i], middle_recv.at[i], pair
        )
        for i in range(steps)
    ]

    def row_copy(k, i):
        src = rows_all.at[2 if k == 2 else 0, step_rows(i), mine]
        dst = rows_all.at[k + 1, step_rows(i), mine]
        return remote(src, dst, row_send.at[k, i], row_recv.at[k, i], {"fs": beside_z if k == 1 else beside_x})

    def forward(k, i):
        ref = rows_all.at[k + 1, step_rows(i), mine]
        return remote(ref, ref, fwd_send.at[k, i], fwd_recv.at[k, i], pair)

    for i in range(steps):
        these = step_rows(i)
        share_copies[i].wait_recv()
        total = part[0, these, mine].astype(f32) + part_in[0, these, :].astype(f32)
        total = total + share_in[these, :].astype(f32)
        middle[these, mine] = (tokens_ref[these, :].astype(f32) + total).astype(bf16)
        middle_copies[i].start()
        middle_copies[i].wait_recv()
        normalize(middle, channel_gain_ref, rows_all.at[0], i * block_size, block_size)
        row_copy(1, i).start()
        row_copy(0, i).start()

    across(0, 1).wait_recv()
    beside(0, 1, 1).start()
    beside(1, 0, 1).start()
    for i in range(steps):
        row_copy(1, i).wait_recv()
        row_copy(2, i).start()
        forward(1, i).start()
        row_copy(0, i).wait_recv()
        forward(0, i).start()
    across(1, 0).wait_recv()
    beside(1, 1, 0).start()
    for g in range(2):
        for b in range(2):
            beside(0, g, b).wait_recv()

    up_tile = sizes["up_tile"]
    unit_base = (2 * zl + x) * units

    def up_product(r):
        @pl.loop(0, units // up_tile)
        def _(j):
            at = span(j * up_tile, up_tile)
            linear = jnp.dot(rows_all[r], up_full[:, at], preferred_element_type=f32)
            linear = linear * up_scale_ref[:, span(unit_base + j * up_tile, up_tile)]
            hidden[r, :, at] = jnp.square(jnp.maximum(linear, 0.0)).astype(bf16)

    up_product(0)
    for k in range(2):
        for i in range(steps):
            forward(k, i).wait_recv()
        up_product(k + 1)
    for i in range(steps):
        row_copy(2, i).wait_recv()
        forward(2, i).start()
    for i in range(steps):
        forward(2, i).wait_recv()
    up_product(3)

    pieces = [(g, b, same) for g in range(2) for same in range(2) for b in range(2)]

    def owner(i):
        return (zh if pieces[i][0] == 0 else 1 - zh) == core

    def term_copy(i):
        return remote(terms.at[i], terms_in.at[i % 4], term_send.at[i % 4], term_recv.at[i % 4], pair)

    def cross_copy(i, k):
        return remote(
            terms.at[i, 2 * k + 1], cross_in.at[i % 4, k], cross_send.at[i % 4, k], cross_recv.at[i % 4, k],
            {"fs": beside_x},
        )

    def line_copy(i):
        return remote(
            terms.at[i, 2], line_in.at[i % 4], line_send.at[i % 4], line_recv.at[i % 4], {"fs": beside_z}
        )

    def columns(i):
        g, b, same = pieces[i]
        yy = y if same == 0 else 1 - y
        return line_of(g, b), yy

    def term_step(i):
        g, b, same = pieces[i]
        if same == 1:
            beside(1, g, b).wait_recv()
        q, yy = columns(i)

        @pl.loop(0, 4)
        def _(r):
            terms[i, r] = jnp.dot(hidden[r], down_full[:, slab_at(q, yy)], preferred_element_type=f32).astype(bf16)

        @pl.when(jnp.logical_not(owner(i)))
        def _():
            term_copy(i).start()

        @pl.when(owner(i))
        def _():
            term_copy(i).wait_recv()

            def add(r):
                @pl.loop(0, rows // fine)
                def _(c):
                    these = span(c * fine, fine, fine)
                    terms[i, r, these, :] = (
                        terms[i, r, these, :].astype(f32) + terms_in[i % 4, r, these, :].astype(f32)
                    ).astype(bf16)

            for r in (3, 1):
                add(r)
                cross_copy(i, r // 2).start()
            for r in (2, 0):
                add(r)

    def cross_step(i):
        @pl.when(owner(i))
        def _():
            cross_copy(i, 1).wait_recv()

            @pl.loop(0, rows // fine)
            def _(c):
                these = span(c * fine, fine, fine)
                terms[i, 2, these, :] = (
                    terms[i, 2, these, :].astype(f32) + cross_in[i % 4, 1, these, :].astype(f32)
                ).astype(bf16)

            line_copy(i).start()
            cross_copy(i, 0).wait_recv()

    def line_step(i):
        g, b, same = pieces[i]
        q, yy = columns(i)

        @pl.when(owner(i))
        def _():
            line_copy(i).wait_recv()
            at = slab_at(q, yy)
            out_at = slab_at(b, yy)

            @pl.loop(0, rows // fine)
            def _(c):
                these = span(c * fine, fine, fine)
                total = terms[i, 0, these, :].astype(f32) + cross_in[i % 4, 0, these, :].astype(f32)
                total = total + line_in[i % 4, these, :].astype(f32)
                out_ref[these, out_at] = (middle[these, at].astype(f32) + total).astype(bf16)

    last = len(pieces) - 1
    for i in range(len(pieces)):
        if i == 2:
            across(1, 1).wait_recv()
            beside(1, 1, 1).start()
        term_step(i)
        if i >= 1:
            cross_step(i - 1)
        if i >= 2:
            line_step(i - 2)
    cross_step(last)
    line_step(last - 1)
    line_step(last)

    for copy in half_copies + sum_copies + part_copies + share_copies + middle_copies:
        copy.wait_send()
    for a in range(2):
        for k in range(3):
            swap(a, k).wait_send()
        for b in range(2):
            across(a, b).wait_send()
            for g in range(2):
                beside(a, g, b).wait_send()
    for q in range(LINES):
        for copy in gate_cross(q, y):
            copy.wait_send()
    for side, step in ((0, 1), (1, -1)):
        for d in range(LINES):
            q = z - step * d

            @pl.when((q >= 0) & (q < LINES) & (z + step >= 0) & (z + step < LINES))
            def _(q=q, side=side, step=step):
                for copy in gate_line(q, side, step):
                    copy.wait_send()

    for k in range(3):
        for i in range(steps):
            row_copy(k, i).wait_send()
            forward(k, i).wait_send()
    for n in range(4):
        for k in range(2):
            cross_copy(n, k).wait_send()
        line_copy(n).wait_send()
        term_copy(n).wait_send()


def fused_shards(fs, tokens, mixer_gain, w_content, w_spatial, content_scale, spatial_scale, spatial_gain,
                 block_mixing, block_bias, w_project, project_scale, channel_gain, w_up, up_scale, w_down, down_scale):
    rows, half = tokens.shape
    width = 2 * half
    channels = w_content.shape[1]
    share_width = channels // 2
    hidden_units = w_up.shape[1]
    units = hidden_units // 4
    depth = w_up.shape[0]
    slab = 2 * depth
    steps = rows // block_mixing.shape[1]
    bf16, f32 = jnp.bfloat16, jnp.float32
    sizes = dict(fine=64, tile=256, up_tile=256)
    vmem = pltpu.VMEM
    dma = pltpu.SemaphoreType.DMA
    row = lambda a: a.reshape(1, -1)
    sems = [(3,), (2,), None, None, (2, 3), (2, 2), (2, 2, 2), (3,), (2,), (steps,), (steps,), (3, steps), (3, steps),
            (4,), (4, 2), (4,)]
    pairs = []
    for shape in sems:
        if shape is not None:
            pairs += [dma(shape), dma(shape)]
        elif len(pairs) == 4:
            pairs += [dma((2, 2, LINES)), dma((2, LINES))]
        else:
            pairs += [dma((2, LINES)), dma((2, LINES))]
    return pl.pallas_call(
        functools.partial(layer_kernel, sizes),
        out_shape=jax.ShapeDtypeStruct((rows, half), bf16),
        in_specs=[
            pl.BlockSpec(memory_space=pl.ANY if i in (12, 14) else vmem) for i in range(16)
        ],
        out_specs=pl.BlockSpec(memory_space=vmem),
        scratch_shapes=[
            vmem((depth, hidden_units), f32),
            vmem((hidden_units, depth), f32),
            dma((2,)),
            vmem((2, rows, width), bf16),
            vmem((2, rows, width), bf16),
            vmem((width, 2 * share_width), bf16),
            vmem((share_width, width), bf16),
            vmem((depth, 2 * share_width), bf16),
            vmem((share_width, depth), bf16),
            vmem((depth, hidden_units), bf16),
            vmem((hidden_units, depth), bf16),
            vmem((width, units), bf16),
            vmem((units, width), bf16),
            vmem((2, rows, share_width), f32),
            vmem((2, rows, share_width), f32),
            vmem((2, rows, share_width), bf16),
            vmem((8, 128), f32),
            vmem((3, 8, 128), f32),
            vmem((2, rows, width), bf16),
            vmem((2, rows, half), bf16),
            vmem((rows, half), bf16),
            vmem((rows, half), bf16),
            vmem((rows, width), bf16),
            vmem((4, rows, width), bf16),
            vmem((4, rows, units), bf16),
            vmem((8, 4, rows, slab), bf16),
            vmem((4, 4, rows, slab), bf16),
            vmem((4, 2, rows, slab), bf16),
            vmem((4, rows, slab), bf16),
        ] + pairs,
        compiler_params=pltpu.CompilerParams(
            collective_id=0, has_side_effects=True, vmem_limit_bytes=VMEM_LIMIT
        ),
    )(tokens, row(mixer_gain), w_content, w_spatial, row(content_scale), row(spatial_scale), row(spatial_gain),
      block_mixing, block_bias, w_project, row(project_scale), row(channel_gain), w_up, row(up_scale), w_down,
      row(down_scale))


VMEM_LIMIT = 67043328


def solution(mesh):
    fs, tp = mesh.shape["fs"], mesh.shape["tp"]
    if tp == 2 and fs == LINES * PLANE:
        body = functools.partial(fused_shards, fs)
    else:
        body = shards
    return jax.shard_map(
        body,
        mesh=mesh,
        in_specs=(
            P("fs", "tp"),
            P(),
            P("fs", "tp"),
            P("fs", "tp"),
            P("tp"),
            P("tp"),
            P("tp"),
            P("tp", None, None),
            P("tp", None),
            P("tp", "fs"),
            P("fs"),
            P(),
            P("fs", "tp"),
            P("tp"),
            P("tp", "fs"),
            P("fs"),
        ),
        out_specs=P("fs", "tp"),
        check_vma=False,
    )
```

time: 204 us -> 201 us (0.985)
  Pallas kernels: 202 us -> 198 us
    pallas_call x1, Pallas kernels: 202 us -> 198 us  [fused_shards(): pl.pallas_call(functools.partial(layer_kernel, sizes), out_shape=jax.Shap...]
where the time goes in v1:
time: 201 us; the launch traced here: 200 us
  Pallas kernels  198 us (99%)
  local copies, waits for them, and re-layouts  2.06 us (1%)
    pallas_call x1, Pallas kernels, fused_shards(): pl.pallas_call(functools.partial(layer_kernel, sizes), out_shape=jax.Shap...  198 us

profile of v1, /device:TPU:1, one launch (start us, length us, event | category | flops | bytes accessed | tf_op | source)
XLA Modules:
  0.0 200.5 jit_solution(6046511501631611662)
XLA Ops:
  0.0 198.4 %shard_map.154 = bf16[384,1024]{1,0:T(8,128)(2,1)} custom-call(bf16[384,1024]{1,0:T(8,128)(2,1)} %tokens_ref.1, f32[1,2048]{1,0:T(1,128)} %bitcast.9, f32[128,512]{1,0:T(8,128)} %content_ref.1, f32[128,512]{1,0:T(8,128)} %spatial_ref.1, f32[1,512]{1,0:T(1,128)} %bitcast.11, f32[1,512]{1,0:T(1,128)} %bitcast.12, f32[1,512]{1,0:T(1,128)} %bitcast.13, ...), custom_call_target="tpu_custom_call" | custom-call | tf_op jit(solution)/shard_map/pallas_call | solution.py:705
  198.4 2.1 %copy.18 = bf16[384,1024]{1,0:T(8,128)(2,1)} copy(bf16[384,1024]{1,0:T(8,128)(2,1)} %shard_map.154) | data formatting | bytes 1572864

commit v2 on v1

--- a/solution.py
+++ b/solution.py
@@ -252,25 +252,37 @@
     def slab_at(q, yy):
         return span((q * PLANE + yy * 2) * depth, slab)
 
-    def gate_refs(q, yy):
-        at = slab_at(q, yy)
+    def gate_refs(q, yy, away):
+        at = span((q * PLANE + yy * 2 + (1 - x if away else x)) * depth, depth)
         return gate_weights.at[at, :], project_full.at[:, at]
 
-    def gate_line(q, side, step):
-        refs = gate_refs(q, y)
+    def gate_line(q, side, step, away):
+        refs = gate_refs(q, y, away)
         return [
             remote(
-                refs[a], refs[a], gate_line_send.at[a, side, q], gate_line_recv.at[a, q],
+                refs[a], refs[a], gate_line_send.at[a, away, side, q], gate_line_recv.at[a, away, q],
                 {"fs": me + step * PLANE},
             )
             for a in range(2)
         ]
 
-    def gate_cross(q, yy):
-        refs = gate_refs(q, yy)
+    def gate_cross(q, yy, away):
+        refs = gate_refs(q, yy, away)
         return [
-            remote(refs[a], refs[a], gate_send.at[a, q], gate_recv.at[a, q], {"fs": beside_y}) for a in range(2)
+            remote(refs[a], refs[a], gate_send.at[a, away, q], gate_recv.at[a, away, q], {"fs": beside_y})
+            for a in range(2)
         ]
+
+    def start_gate(away):
+        for side, step in ((0, 1), (1, -1)):
+
+            @pl.when((z + step >= 0) & (z + step < LINES))
+            def _(side=side, step=step):
+                for copy in gate_line(z, side, step, away):
+                    copy.start()
+
+        for copy in gate_cross(z, y, away):
+            copy.start()
 
     half_copies = [
         remote(gate_other, gate_weights.at[own_depth, :], half_send.at[0], half_recv.at[0], {"fs": beside_x}),
@@ -300,25 +312,26 @@
         ref = ff_ref(a, line_of(g, b), y)
         return remote(ref, ref, beside_send.at[a, g, b], beside_recv.at[a, g, b], {"fs": beside_y})
 
-    def relay_gate(d):
+    def relay_gate(d, away):
         for side, step in ((0, 1), (1, -1)):
             q = z - step * d
 
             @pl.when((q >= 0) & (q < LINES))
             def _(q=q, side=side, step=step):
-                for copy in gate_line(q, side, step):
+                for copy in gate_line(q, side, step, away):
                     copy.wait_recv()
 
                 @pl.when((z + step >= 0) & (z + step < LINES))
                 def _():
-                    for copy in gate_line(q, side, step):
+                    for copy in gate_line(q, side, step, away):
                         copy.start()
 
-                for copy in gate_cross(q, y):
+                for copy in gate_cross(q, y, away):
                     copy.start()
 
     for copy in half_copies:
         copy.start()
+    start_gate(0)
     token_pair = remote(tokens_ref, token_rows.at[0, :, mine], token_send.at[0], token_recv.at[0], pair)
     token_pair.start()
     for load in loads:
@@ -346,17 +359,12 @@
 
     for copy in half_copies:
         copy.wait_recv()
-    for side, step in ((0, 1), (1, -1)):
-
-        @pl.when((z + step >= 0) & (z + step < LINES))
-        def _(side=side, step=step):
-            for copy in gate_line(z, side, step):
-                copy.start()
-
-    for copy in gate_cross(z, y):
-        copy.start()
-    swap(0, 1).start()
-    swap(0, 2).start()
+    start_gate(1)
+
+    @pl.when(jnp.logical_not(inner))
+    def _():
+        swap(0, 1).start()
+        swap(0, 2).start()
 
     def normalize(source, gain_ref, target, first, count):
         @pl.loop(0, count // fine)
@@ -368,19 +376,32 @@
 
     token_pair.wait()
     normalize(token_rows.at[0], mixer_gain_ref, normed.at[0], 0, rows)
-    relay_gate(1)
-    relay_gate(2)
-    for k in range(3):
-        swap(1, k).start()
-    for k in range(3):
-        swap(0, k).wait_recv()
-    for b in range(2):
-        across(0, b).start()
-    relay_gate(3)
-    for b in range(2):
-        beside(0, 0, b).start()
-
+    relay_gate(1, 0)
+    relay_gate(1, 1)
+    swap(0, 0).wait_recv()
+    relay_gate(2, 0)
+    relay_gate(2, 1)
+
+    @pl.when(inner)
+    def _():
+        swap(0, 1).start()
+        swap(0, 2).start()
+
+    @pl.when(jnp.logical_not(inner))
+    def _():
+        across(0, zl).start()
+
+    swap(1, 0).start()
+    relay_gate(3, 0)
+    relay_gate(3, 1)
+    beside(0, 0, zl).start()
     token_cross.wait()
+
+    @pl.when(inner)
+    def _():
+        across(0, zl).start()
+
+
     token_forward = remote(
         token_rows.at[1, :, mine], token_rows.at[1, :, mine], token_send.at[2], token_recv.at[2], pair
     )
@@ -388,9 +409,35 @@
     token_forward.wait()
     normalize(token_rows.at[1], mixer_gain_ref, normed.at[1], 0, rows)
 
+    def finish_up_swap():
+        swap(0, 1).wait_recv()
+        swap(0, 2).wait_recv()
+        across(0, 1 - zl).start()
+        beside(0, 0, 1 - zl).start()
+
+    @pl.when(inner)
+    def _():
+        finish_up_swap()
+
+    swap(1, 1).start()
+    swap(1, 2).start()
+    swap(1, 0).wait_recv()
+
+    @pl.when(jnp.logical_not(inner))
+    def _():
+        across(1, zl).start()
+
+    beside(1, 0, zl).start()
+
+    def finish_down_swap():
+        swap(1, 1).wait_recv()
+        swap(1, 2).wait_recv()
+        across(1, 1 - zl).start()
+
     for q in range(LINES):
-        for copy in gate_cross(q, 1 - y):
-            copy.wait_recv()
+        for away in range(2):
+            for copy in gate_cross(q, 1 - y, away):
+                copy.wait_recv()
 
     @pl.loop(0, 2)
     def _(s):
@@ -468,14 +515,6 @@
         share_copies[i].start()
     part_copies[0].wait_recv()
 
-    for k in range(3):
-        swap(1, k).wait_recv()
-    for b in range(2):
-        across(1, b).start()
-    across(0, 0).wait_recv()
-    beside(0, 1, 0).start()
-    beside(1, 0, 0).start()
-
     middle_copies = [
         remote(
             middle.at[step_rows(i), mine], middle.at[step_rows(i), mine], middle_send.at[i], middle_recv.at[i], pair
@@ -491,6 +530,10 @@
     def forward(k, i):
         ref = rows_all.at[k + 1, step_rows(i), mine]
         return remote(ref, ref, fwd_send.at[k, i], fwd_recv.at[k, i], pair)
+
+    @pl.when(jnp.logical_not(inner))
+    def _():
+        finish_up_swap()
 
     for i in range(steps):
         these = step_rows(i)
@@ -503,18 +546,51 @@
         normalize(middle, channel_gain_ref, rows_all.at[0], i * block_size, block_size)
         row_copy(1, i).start()
         row_copy(0, i).start()
-
-    across(0, 1).wait_recv()
-    beside(0, 1, 1).start()
-    beside(1, 0, 1).start()
+        if i == steps - 2:
+            across(0, zl).wait_recv()
+            beside(0, 1, zl).start()
+
+    def pass_on(a, b):
+        across(a, b).wait_recv()
+        beside(a, 1, b).start()
+
+    @pl.when(jnp.logical_not(inner))
+    def _():
+        pass_on(0, 1 - zl)
+
     for i in range(steps):
         row_copy(1, i).wait_recv()
         row_copy(2, i).start()
         forward(1, i).start()
+        if i == 0:
+
+            @pl.when(jnp.logical_not(inner))
+            def _():
+                finish_down_swap()
+
+            @pl.when(inner)
+            def _():
+                pass_on(0, 1 - zl)
+
+        if i == steps - 2:
+
+            @pl.when(inner)
+            def _():
+                across(1, zl).start()
+
+    @pl.when(inner)
+    def _():
+        finish_down_swap()
+
+    beside(1, 0, 1 - zl).start()
+
+    @pl.when(inner)
+    def _():
+        pass_on(1, zl)
+
+    for i in range(steps):
         row_copy(0, i).wait_recv()
         forward(0, i).start()
-    across(1, 0).wait_recv()
-    beside(1, 1, 0).start()
     for g in range(2):
         for b in range(2):
             beside(0, g, b).wait_recv()
@@ -535,114 +611,161 @@
         for i in range(steps):
             forward(k, i).wait_recv()
         up_product(k + 1)
+
+    @pl.when(jnp.logical_not(inner))
+    def _():
+        pass_on(1, zl)
+
+    @pl.when(inner)
+    def _():
+        pass_on(1, 1 - zl)
+
+
+    pieces = [(g, same, late) for g in range(2) for same in range(2) for late in range(2)]
+
+    def bit(i):
+        g, same, late = pieces[i]
+        if g == 0 or same == 0:
+            return late
+        return zl if late == 0 else 1 - zl
+
+    def place(i):
+        g, same, _ = pieces[i]
+        n = 2 * same + bit(i)
+        return 4 * g + n, n
+
+    def columns(i):
+        g, same, _ = pieces[i]
+        return line_of(g, bit(i)), y if same == 0 else 1 - y
+
+    def owner(i):
+        return (zh if pieces[i][0] == 0 else 1 - zh) == core
+
+    def term_copy(i, k):
+        at, n = place(i)
+        src, dst = (terms.at[at, 3], terms_in.at[n, 3]) if k else (terms.at[at, 0:3], terms_in.at[n, 0:3])
+        return remote(src, dst, term_send.at[n, k], term_recv.at[n, k], pair)
+
+    def routes(i):
+        return (1, beside_x, 2, beside_z) if pieces[i][0] == 0 else (2, beside_z, 1, beside_x)
+
+    def cross_copy(i, k):
+        at, n = place(i)
+        slot, to, _, _ = routes(i)
+        src = terms.at[at, 3 if k else slot]
+        return remote(src, cross_in.at[n, k], cross_send.at[n, k], cross_recv.at[n, k], {"fs": to})
+
+    def line_copy(i):
+        at, n = place(i)
+        _, _, slot, to = routes(i)
+        return remote(terms.at[at, slot], line_in.at[n], line_send.at[n], line_recv.at[n], {"fs": to})
+
+    def product_step(i, k):
+        g, same, _ = pieces[i]
+        if same == 1 and k == 0:
+            beside(1, g, bit(i)).wait_recv()
+        at, _ = place(i)
+        q, yy = columns(i)
+
+        def product(r):
+            terms[at, r] = jnp.dot(hidden[r], down_full[:, slab_at(q, yy)], preferred_element_type=f32).astype(bf16)
+
+        if k == 0:
+            pl.loop(0, 3)(product)
+        else:
+            product(3)
+
+        @pl.when(jnp.logical_not(owner(i)))
+        def _():
+            term_copy(i, k).start()
+
+    def add_step(i, k):
+        at, n = place(i)
+
+        @pl.when(owner(i))
+        def _():
+            term_copy(i, k).wait_recv()
+
+            def add(r):
+                @pl.loop(0, rows // fine)
+                def _(c):
+                    these = span(c * fine, fine, fine)
+                    terms[at, r, these, :] = (
+                        terms[at, r, these, :].astype(f32) + terms_in[n, r, these, :].astype(f32)
+                    ).astype(bf16)
+
+            first, _, second, _ = routes(i)
+            if k == 1:
+                add(3)
+                cross_copy(i, 1).start()
+            else:
+                add(first)
+                cross_copy(i, 0).start()
+                add(second)
+                add(0)
+
+    def cross_step(i):
+        at, n = place(i)
+
+        @pl.when(owner(i))
+        def _():
+            cross_copy(i, 1).wait_recv()
+            slot = routes(i)[2]
+
+            @pl.loop(0, rows // fine)
+            def _(c):
+                these = span(c * fine, fine, fine)
+                terms[at, slot, these, :] = (
+                    terms[at, slot, these, :].astype(f32) + cross_in[n, 1, these, :].astype(f32)
+                ).astype(bf16)
+
+            line_copy(i).start()
+            cross_copy(i, 0).wait_recv()
+
+    def line_step(i):
+        at, n = place(i)
+        q, yy = columns(i)
+
+        @pl.when(owner(i))
+        def _():
+            line_copy(i).wait_recv()
+            out_at = slab_at(q % 2, yy)
+
+            @pl.loop(0, rows // fine)
+            def _(c):
+                these = span(c * fine, fine, fine)
+                total = terms[at, 0, these, :].astype(f32) + cross_in[n, 0, these, :].astype(f32)
+                total = total + line_in[n, these, :].astype(f32)
+                out_ref[these, out_at] = (middle[these, slab_at(q, yy)].astype(f32) + total).astype(bf16)
+
+    def far_step(i):
+        @pl.when(jnp.logical_not(inner))
+        def _():
+            pass_on(1, 1 - zl)
+
+    def run_tail(names):
+        kinds = dict(
+            p=lambda i: (product_step(i, 0), product_step(i, 1)),
+            q=lambda i: product_step(i, 0),
+            r=lambda i: product_step(i, 1),
+            a=lambda i: (add_step(i, 0), add_step(i, 1)),
+            b=lambda i: add_step(i, 0),
+            d=lambda i: add_step(i, 1),
+            c=cross_step,
+            l=line_step,
+            f=far_step,
+        )
+        for name in names:
+            kinds[name[0]](int(name[1]))
+
+    run_tail(sizes["early"])
     for i in range(steps):
         row_copy(2, i).wait_recv()
         forward(2, i).start()
     for i in range(steps):
         forward(2, i).wait_recv()
     up_product(3)
-
-    pieces = [(g, b, same) for g in range(2) for same in range(2) for b in range(2)]
-
-    def owner(i):
-        return (zh if pieces[i][0] == 0 else 1 - zh) == core
-
-    def term_copy(i):
-        return remote(terms.at[i], terms_in.at[i % 4], term_send.at[i % 4], term_recv.at[i % 4], pair)
-
-    def cross_copy(i, k):
-        return remote(
-            terms.at[i, 2 * k + 1], cross_in.at[i % 4, k], cross_send.at[i % 4, k], cross_recv.at[i % 4, k],
-            {"fs": beside_x},
-        )
-
-    def line_copy(i):
-        return remote(
-            terms.at[i, 2], line_in.at[i % 4], line_send.at[i % 4], line_recv.at[i % 4], {"fs": beside_z}
-        )
-
-    def columns(i):
-        g, b, same = pieces[i]
-        yy = y if same == 0 else 1 - y
-        return line_of(g, b), yy
-
-    def term_step(i):
-        g, b, same = pieces[i]
-        if same == 1:
-            beside(1, g, b).wait_recv()
-        q, yy = columns(i)
-
-        @pl.loop(0, 4)
-        def _(r):
-            terms[i, r] = jnp.dot(hidden[r], down_full[:, slab_at(q, yy)], preferred_element_type=f32).astype(bf16)
-
-        @pl.when(jnp.logical_not(owner(i)))
-        def _():
-            term_copy(i).start()
-
-        @pl.when(owner(i))
-        def _():
-            term_copy(i).wait_recv()
-
-            def add(r):
-                @pl.loop(0, rows // fine)
-                def _(c):
-                    these = span(c * fine, fine, fine)
-                    terms[i, r, these, :] = (
-                        terms[i, r, these, :].astype(f32) + terms_in[i % 4, r, these, :].astype(f32)
-                    ).astype(bf16)
-
-            for r in (3, 1):
-                add(r)
-                cross_copy(i, r // 2).start()
-            for r in (2, 0):
-                add(r)
-
-    def cross_step(i):
-        @pl.when(owner(i))
-        def _():
-            cross_copy(i, 1).wait_recv()
-
-            @pl.loop(0, rows // fine)
-            def _(c):
-                these = span(c * fine, fine, fine)
-                terms[i, 2, these, :] = (
-                    terms[i, 2, these, :].astype(f32) + cross_in[i % 4, 1, these, :].astype(f32)
-                ).astype(bf16)
-
-            line_copy(i).start()
-            cross_copy(i, 0).wait_recv()
-
-    def line_step(i):
-        g, b, same = pieces[i]
-        q, yy = columns(i)
-
-        @pl.when(owner(i))
-        def _():
-            line_copy(i).wait_recv()
-            at = slab_at(q, yy)
-            out_at = slab_at(b, yy)
-
-            @pl.loop(0, rows // fine)
-            def _(c):
-                these = span(c * fine, fine, fine)
-                total = terms[i, 0, these, :].astype(f32) + cross_in[i % 4, 0, these, :].astype(f32)
-                total = total + line_in[i % 4, these, :].astype(f32)
-                out_ref[these, out_at] = (middle[these, at].astype(f32) + total).astype(bf16)
-
-    last = len(pieces) - 1
-    for i in range(len(pieces)):
-        if i == 2:
-            across(1, 1).wait_recv()
-            beside(1, 1, 1).start()
-        term_step(i)
-        if i >= 1:
-            cross_step(i - 1)
-        if i >= 2:
-            line_step(i - 2)
-    cross_step(last)
-    line_step(last - 1)
-    line_step(last)
+    run_tail(sizes["late"])
 
     for copy in half_copies + sum_copies + part_copies + share_copies + middle_copies:
         copy.wait_send()
@@ -654,26 +777,29 @@
             for g in range(2):
                 beside(a, g, b).wait_send()
     for q in range(LINES):
-        for copy in gate_cross(q, y):
-            copy.wait_send()
+        for away in range(2):
+            for copy in gate_cross(q, y, away):
+                copy.wait_send()
     for side, step in ((0, 1), (1, -1)):
         for d in range(LINES):
             q = z - step * d
 
             @pl.when((q >= 0) & (q < LINES) & (z + step >= 0) & (z + step < LINES))
             def _(q=q, side=side, step=step):
-                for copy in gate_line(q, side, step):
-                    copy.wait_send()
+                for away in range(2):
+                    for copy in gate_line(q, side, step, away):
+                        copy.wait_send()
 
     for k in range(3):
         for i in range(steps):
             row_copy(k, i).wait_send()
             forward(k, i).wait_send()
-    for n in range(4):
+    for i in range(4):
         for k in range(2):
-            cross_copy(n, k).wait_send()
-        line_copy(n).wait_send()
-        term_copy(n).wait_send()
+            cross_copy(i, k).wait_send()
+        line_copy(i).wait_send()
+        for k in range(2):
+            term_copy(i, k).wait_send()
 
 
 def fused_shards(fs, tokens, mixer_gain, w_content, w_spatial, content_scale, spatial_scale, spatial_gain,
@@ -688,20 +814,28 @@
     slab = 2 * depth
     steps = rows // block_mixing.shape[1]
     bf16, f32 = jnp.bfloat16, jnp.float32
-    sizes = dict(fine=64, tile=256, up_tile=256)
+    early = [
+        "q0", "q2",
+    ]
+    late = [
+        "r0", "b0", "r2", "d0", "f1", "p4", "b2", "d2", "p5", "a4", "p1", "a5", "p3", "a1", "p6", "a3", "c0",
+        "a6", "c4", "c2", "p7", "a7", "c5", "c1", "c6", "c3", "c7", "l0", "l2", "l4", "l5", "l1", "l3", "l6",
+        "l7",
+    ]
+    sizes = dict(fine=64, tile=256, up_tile=256, early=early, late=late)
     vmem = pltpu.VMEM
     dma = pltpu.SemaphoreType.DMA
     row = lambda a: a.reshape(1, -1)
     sems = [(3,), (2,), None, None, (2, 3), (2, 2), (2, 2, 2), (3,), (2,), (steps,), (steps,), (3, steps), (3, steps),
-            (4,), (4, 2), (4,)]
+            (4, 2), (4, 2), (4,)]
     pairs = []
     for shape in sems:
         if shape is not None:
             pairs += [dma(shape), dma(shape)]
         elif len(pairs) == 4:
-            pairs += [dma((2, 2, LINES)), dma((2, LINES))]
+            pairs += [dma((2, 2, 2, LINES)), dma((2, 2, LINES))]
         else:
-            pairs += [dma((2, LINES)), dma((2, LINES))]
+            pairs += [dma((2, 2, LINES)), dma((2, 2, LINES))]
     return pl.pallas_call(
         functools.partial(layer_kernel, sizes),
         out_shape=jax.ShapeDtypeStruct((rows, half), bf16),

time: 201 us -> 163 us (0.81)
  Pallas kernels: 198 us -> 159 us
    pallas_call x1, Pallas kernels: 198 us -> 159 us  [fused_shards(): pl.pallas_call(functools.partial(layer_kernel, sizes), out_shape=jax.Shap...]
where the time goes in v2:
time: 163 us; the launch traced here: 161 us
  Pallas kernels  159 us (98%)
  local copies, waits for them, and re-layouts  2.06 us (1%)
    pallas_call x1, Pallas kernels, fused_shards(): pl.pallas_call(functools.partial(layer_kernel, sizes), out_shape=jax.Shap...  159 us

profile of v2, /device:TPU:1, one launch (start us, length us, event | category | flops | bytes accessed | tf_op | source)
XLA Modules:
  0.0 161.2 jit_solution(7900554050327821044)
XLA Ops:
  0.0 159.2 %shard_map.154 = bf16[384,1024]{1,0:T(8,128)(2,1)} custom-call(bf16[384,1024]{1,0:T(8,128)(2,1)} %tokens_ref.1, f32[1,2048]{1,0:T(1,128)} %bitcast.9, f32[128,512]{1,0:T(8,128)} %content_ref.1, f32[128,512]{1,0:T(8,128)} %spatial_ref.1, f32[1,512]{1,0:T(1,128)} %bitcast.11, f32[1,512]{1,0:T(1,128)} %bitcast.12, f32[1,512]{1,0:T(1,128)} %bitcast.13, ...), custom_call_target="tpu_custom_call" | custom-call | tf_op jit(solution)/shard_map/pallas_call | solution.py:839
  159.2 2.1 %copy.18 = bf16[384,1024]{1,0:T(8,128)(2,1)} copy(bf16[384,1024]{1,0:T(8,128)(2,1)} %shard_map.154) | data formatting | bytes 1572864

commit v3 on v2

--- a/solution.py
+++ b/solution.py
@@ -647,7 +647,7 @@
         return remote(src, dst, term_send.at[n, k], term_recv.at[n, k], pair)
 
     def routes(i):
-        return (1, beside_x, 2, beside_z) if pieces[i][0] == 0 else (2, beside_z, 1, beside_x)
+        return (2, beside_z, 1, beside_x) if i in (3, 4, 5) else (1, beside_x, 2, beside_z)
 
     def cross_copy(i, k):
         at, n = place(i)
@@ -660,10 +660,13 @@
         _, _, slot, to = routes(i)
         return remote(terms.at[at, slot], line_in.at[n], line_send.at[n], line_recv.at[n], {"fs": to})
 
+    arrived = set()
+
     def product_step(i, k):
         g, same, _ = pieces[i]
-        if same == 1 and k == 0:
+        if same == 1 and i not in arrived:
             beside(1, g, bit(i)).wait_recv()
+        arrived.add(i)
         at, _ = place(i)
         q, yy = columns(i)
 
@@ -745,10 +748,10 @@
 
     def run_tail(names):
         kinds = dict(
-            p=lambda i: (product_step(i, 0), product_step(i, 1)),
+            p=lambda i: (product_step(i, 1), product_step(i, 0)),
             q=lambda i: product_step(i, 0),
             r=lambda i: product_step(i, 1),
-            a=lambda i: (add_step(i, 0), add_step(i, 1)),
+            a=lambda i: (add_step(i, 1), add_step(i, 0)),
             b=lambda i: add_step(i, 0),
             d=lambda i: add_step(i, 1),
             c=cross_step,
@@ -815,12 +818,11 @@
     steps = rows // block_mixing.shape[1]
     bf16, f32 = jnp.bfloat16, jnp.float32
     early = [
-        "q0", "q2",
+        "q0", "q2", "b0", "b2",
     ]
     late = [
-        "r0", "b0", "r2", "d0", "f1", "p4", "b2", "d2", "p5", "a4", "p1", "a5", "p3", "a1", "p6", "a3", "c0",
-        "a6", "c4", "c2", "p7", "a7", "c5", "c1", "c6", "c3", "c7", "l0", "l2", "l4", "l5", "l1", "l3", "l6",
-        "l7",
+        "r0", "r2", "d0", "f1", "p4", "d2", "p5", "a4", "p1", "a5", "p6", "a1", "p3", "a6", "c0", "a3", "c2",
+        "p7", "a7", "c4", "c5", "c1", "c6", "c3", "c7", "l0", "l2", "l4", "l5", "l1", "l3", "l6", "l7",
     ]
     sizes = dict(fine=64, tile=256, up_tile=256, early=early, late=late)
     vmem = pltpu.VMEM

time: 163 us -> 156 us (0.957); the launches traced: 161 us -> 156 us
  Pallas kernels: 159 us -> 154 us
    pallas_call x1, Pallas kernels: 159 us -> 154 us  [fused_shards(): pl.pallas_call(functools.partial(layer_kernel, sizes), out_shape=jax.Shap...]
where the time goes in v3:
time: 156 us
  Pallas kernels  154 us (99%)
  local copies, waits for them, and re-layouts  2.06 us (1%)
    pallas_call x1, Pallas kernels, fused_shards(): pl.pallas_call(functools.partial(layer_kernel, sizes), out_shape=jax.Shap...  154 us

profile of v3, /device:TPU:1, one launch (start us, length us, event | category | flops | bytes accessed | tf_op | source)
XLA Modules:
  0.0 156.0 jit_solution(15001070790506004700)
XLA Ops:
  0.0 153.9 %shard_map.154 = bf16[384,1024]{1,0:T(8,128)(2,1)} custom-call(bf16[384,1024]{1,0:T(8,128)(2,1)} %tokens_ref.1, f32[1,2048]{1,0:T(1,128)} %bitcast.9, f32[128,512]{1,0:T(8,128)} %content_ref.1, f32[128,512]{1,0:T(8,128)} %spatial_ref.1, f32[1,512]{1,0:T(1,128)} %bitcast.11, f32[1,512]{1,0:T(1,128)} %bitcast.12, f32[1,512]{1,0:T(1,128)} %bitcast.13, ...), custom_call_target="tpu_custom_call" | custom-call | tf_op jit(solution)/shard_map/pallas_call | solution.py:841
  154.0 2.1 %copy.18 = bf16[384,1024]{1,0:T(8,128)(2,1)} copy(bf16[384,1024]{1,0:T(8,128)(2,1)} %shard_map.154) | data formatting | bytes 1572864

commit v4 on v3

--- a/solution.py
+++ b/solution.py
@@ -98,6 +98,23 @@
 
 def layer_kernel(
     sizes,
+    tokens_hbm,
+    mixer_gain_hbm,
+    content_hbm,
+    spatial_hbm,
+    content_scale_hbm,
+    spatial_scale_hbm,
+    spatial_gain_hbm,
+    mixing_hbm,
+    bias_hbm,
+    project_hbm,
+    project_scale_hbm,
+    channel_gain_hbm,
+    up_hbm,
+    up_scale_hbm,
+    down_hbm,
+    down_scale_hbm,
+    out_ref,
     tokens_ref,
     mixer_gain_ref,
     content_ref,
@@ -110,13 +127,10 @@
     project_ref,
     project_scale_ref,
     channel_gain_ref,
-    up_hbm,
+    up_ref,
     up_scale_ref,
-    down_hbm,
+    down_ref,
     down_scale_ref,
-    out_ref,
-    up_ref,
-    down_ref,
     load_sem,
     token_rows,
     normed,
@@ -217,10 +231,25 @@
             src_ref=src, dst_ref=dst, send_sem=send, recv_sem=recv, device_id=where, device_id_type=MESH
         )
 
-    loads = [
-        pltpu.make_async_copy(up_hbm, up_ref, load_sem.at[0]),
-        pltpu.make_async_copy(down_hbm, down_ref, load_sem.at[1]),
+    staged = [
+        (content_hbm, content_ref),
+        (spatial_hbm, spatial_ref),
+        (project_hbm, project_ref),
+        (project_scale_hbm, project_scale_ref),
+        (tokens_hbm, tokens_ref),
+        (up_hbm, up_ref),
+        (down_hbm, down_ref),
+        (down_scale_hbm, down_scale_ref),
+        (mixer_gain_hbm, mixer_gain_ref),
+        (content_scale_hbm, content_scale_ref),
+        (spatial_scale_hbm, spatial_scale_ref),
+        (spatial_gain_hbm, spatial_gain_ref),
+        (mixing_hbm, mixing_ref),
+        (bias_hbm, bias_ref),
+        (channel_gain_hbm, channel_gain_ref),
+        (up_scale_hbm, up_scale_ref),
     ]
+    loads = [pltpu.make_async_copy(src, dst, load_sem.at[i]) for i, (src, dst) in enumerate(staged)]
     for load in loads:
         load.start()
     barrier = pltpu.get_barrier_semaphore()
@@ -244,8 +273,11 @@
         weights[:, pl.ds(share_width, share_width)] = spatial_ref[:, at].astype(bf16)
         project[...] = (project_ref[at, :] * project_scale_ref[...]).astype(bf16)
 
+    for load in loads[:4]:
+        load.wait()
     halves(1 - x, gate_other, project_other)
     halves(x, gate_weights.at[own_depth, :], project_full.at[:, own_depth])
+    loads[4].wait()
     token_rows[0, :, mine] = tokens_ref[...]
     pl.semaphore_wait(barrier, len(friends) + inner.astype(jnp.int32))
 
@@ -334,7 +366,7 @@
     start_gate(0)
     token_pair = remote(tokens_ref, token_rows.at[0, :, mine], token_send.at[0], token_recv.at[0], pair)
     token_pair.start()
-    for load in loads:
+    for load in loads[5:]:
         load.wait()
 
     @pl.loop(0, up_own.shape[1] // units)
@@ -828,6 +860,11 @@
     vmem = pltpu.VMEM
     dma = pltpu.SemaphoreType.DMA
     row = lambda a: a.reshape(1, -1)
+    operands = (
+        tokens, row(mixer_gain), w_content, w_spatial, row(content_scale), row(spatial_scale), row(spatial_gain),
+        block_mixing, block_bias, w_project, row(project_scale), row(channel_gain), w_up, row(up_scale), w_down,
+        row(down_scale),
+    )
     sems = [(3,), (2,), None, None, (2, 3), (2, 2), (2, 2, 2), (3,), (2,), (steps,), (steps,), (3, steps), (3, steps),
             (4, 2), (4, 2), (4,)]
     pairs = []
@@ -842,13 +879,12 @@
         functools.partial(layer_kernel, sizes),
         out_shape=jax.ShapeDtypeStruct((rows, half), bf16),
         in_specs=[
-            pl.BlockSpec(memory_space=pl.ANY if i in (12, 14) else vmem) for i in range(16)
+            pl.BlockSpec(memory_space=pl.ANY) for _ in range(16)
         ],
         out_specs=pl.BlockSpec(memory_space=vmem),
         scratch_shapes=[
-            vmem((depth, hidden_units), f32),
-            vmem((hidden_units, depth), f32),
-            dma((2,)),
+            *[vmem(a.shape, a.dtype) for a in operands],
+            dma((len(operands),)),
             vmem((2, rows, width), bf16),
             vmem((2, rows, width), bf16),
             vmem((width, 2 * share_width), bf16),
@@ -879,9 +915,7 @@
         compiler_params=pltpu.CompilerParams(
             collective_id=0, has_side_effects=True, vmem_limit_bytes=VMEM_LIMIT
         ),
-    )(tokens, row(mixer_gain), w_content, w_spatial, row(content_scale), row(spatial_scale), row(spatial_gain),
-      block_mixing, block_bias, w_project, row(project_scale), row(channel_gain), w_up, row(up_scale), w_down,
-      row(down_scale))
+    )(*operands)
 
 
 VMEM_LIMIT = 67043328

time: 156 us -> 155 us (level)
  no operation moved by 1% of the time
where the time goes in v4:
time: 155 us
  Pallas kernels  153 us (99%)
  local copies, waits for them, and re-layouts  2.06 us (1%)
    pallas_call x1, Pallas kernels, fused_shards(): pl.pallas_call(functools.partial(layer_kernel, sizes), out_shape=jax.Shap...  153 us

profile of v4, /device:TPU:1, one launch (start us, length us, event | category | flops | bytes accessed | tf_op | source)
XLA Modules:
  0.0 154.6 jit_solution(16949974888688487840)
XLA Ops:
  0.0 152.6 %shard_map.154 = bf16[384,1024]{1,0:T(8,128)(2,1)} custom-call(bf16[384,1024]{1,0:T(8,128)(2,1)} %tokens_hbm.1, f32[1,2048]{1,0:T(1,128)} %bitcast.9, f32[128,512]{1,0:T(8,128)} %content_hbm.1, f32[128,512]{1,0:T(8,128)} %spatial_hbm.1, f32[1,512]{1,0:T(1,128)} %bitcast.11, f32[1,512]{1,0:T(1,128)} %bitcast.12, f32[1,512]{1,0:T(1,128)} %bitcast.13, ...), custom_call_target="tpu_custom_call" | custom-call | tf_op jit(solution)/shard_map/pallas_call | solution.py:878
  152.6 2.1 %copy.18 = bf16[384,1024]{1,0:T(8,128)(2,1)} copy(bf16[384,1024]{1,0:T(8,128)(2,1)} %shard_map.154) | data formatting | bytes 1572864

commit v5 on v4

--- a/solution.py
+++ b/solution.py
@@ -114,7 +114,7 @@
     up_scale_hbm,
     down_hbm,
     down_scale_hbm,
-    out_ref,
+    out_hbm,
     tokens_ref,
     mixer_gain_ref,
     content_ref,
@@ -190,6 +190,8 @@
     cross_recv,
     line_send,
     line_recv,
+    out_ref,
+    out_sem,
 ):
     rows, half = tokens_ref.shape
     width = 2 * half
@@ -757,6 +759,11 @@
             line_copy(i).start()
             cross_copy(i, 0).wait_recv()
 
+    def out_copy(i):
+        q, yy = columns(i)
+        cols = slab_at(q % 2, yy)
+        return pltpu.make_async_copy(out_ref.at[:, cols], out_hbm.at[:, cols], out_sem.at[place(i)[1]])
+
     def line_step(i):
         at, n = place(i)
         q, yy = columns(i)
@@ -772,6 +779,8 @@
                 total = terms[at, 0, these, :].astype(f32) + cross_in[n, 0, these, :].astype(f32)
                 total = total + line_in[n, these, :].astype(f32)
                 out_ref[these, out_at] = (middle[these, slab_at(q, yy)].astype(f32) + total).astype(bf16)
+
+            out_copy(i).start()
 
     def far_step(i):
         @pl.when(jnp.logical_not(inner))
@@ -829,6 +838,12 @@
         for i in range(steps):
             row_copy(k, i).wait_send()
             forward(k, i).wait_send()
+    for i in range(8):
+
+        @pl.when(owner(i))
+        def _(i=i):
+            out_copy(i).wait()
+
     for i in range(4):
         for k in range(2):
             cross_copy(i, k).wait_send()
@@ -856,7 +871,7 @@
         "r0", "r2", "d0", "f1", "p4", "d2", "p5", "a4", "p1", "a5", "p6", "a1", "p3", "a6", "c0", "a3", "c2",
         "p7", "a7", "c4", "c5", "c1", "c6", "c3", "c7", "l0", "l2", "l4", "l5", "l1", "l3", "l6", "l7",
     ]
-    sizes = dict(fine=64, tile=256, up_tile=256, early=early, late=late)
+    sizes = dict(fine=128, tile=256, up_tile=256, early=early, late=late)
     vmem = pltpu.VMEM
     dma = pltpu.SemaphoreType.DMA
     row = lambda a: a.reshape(1, -1)
@@ -881,7 +896,7 @@
         in_specs=[
             pl.BlockSpec(memory_space=pl.ANY) for _ in range(16)
         ],
-        out_specs=pl.BlockSpec(memory_space=vmem),
+        out_specs=pl.BlockSpec(memory_space=pl.ANY),
         scratch_shapes=[
             *[vmem(a.shape, a.dtype) for a in operands],
             dma((len(operands),)),
@@ -911,7 +926,7 @@
             vmem((4, 4, rows, slab), bf16),
             vmem((4, 2, rows, slab), bf16),
             vmem((4, rows, slab), bf16),
-        ] + pairs,
+        ] + pairs + [vmem((rows, half), bf16), dma((4,))],
         compiler_params=pltpu.CompilerParams(
             collective_id=0, has_side_effects=True, vmem_limit_bytes=VMEM_LIMIT
         ),

time: 155 us -> 154 us (level)
  no operation moved by 1% of the time
where the time goes in v5:
time: 154 us
  Pallas kernels  152 us (99%)
  local copies, waits for them, and re-layouts  2.06 us (1%)
    pallas_call x1, Pallas kernels, fused_shards(): pl.pallas_call(functools.partial(layer_kernel, sizes), out_shape=jax.Shap...  152 us

profile of v5, /device:TPU:1, one launch (start us, length us, event | category | flops | bytes accessed | tf_op | source)
XLA Modules:
  0.0 153.9 jit_solution(8455568818464208638)
XLA Ops:
  0.0 151.8 %shard_map.154 = bf16[384,1024]{1,0:T(8,128)(2,1)} custom-call(bf16[384,1024]{1,0:T(8,128)(2,1)} %tokens_hbm.1, f32[1,2048]{1,0:T(1,128)} %bitcast.9, f32[128,512]{1,0:T(8,128)} %content_hbm.1, f32[128,512]{1,0:T(8,128)} %spatial_hbm.1, f32[1,512]{1,0:T(1,128)} %bitcast.11, f32[1,512]{1,0:T(1,128)} %bitcast.12, f32[1,512]{1,0:T(1,128)} %bitcast.13, ...), custom_call_target="tpu_custom_call" | custom-call | tf_op jit(solution)/shard_map/pallas_call | solution.py:893
  151.8 2.1 %copy.18 = bf16[384,1024]{1,0:T(8,128)(2,1)} copy(bf16[384,1024]{1,0:T(8,128)(2,1)} %shard_map.154) | data formatting | bytes 1572864
